TPU v7x, 32 devices: a whole 2x2x4 slice. The times are simulated.
32 devices in a mesh: ep: 8 (over z, y), tp: 4 (over x, core).
Axes of the slice: x: 2, y: 2, z: 4, core: 2. Of those that a mesh axis runs over, the one named last changes fastest.
Arguments:
- tokens: bfloat16 [128, 1024], P('ep'), may hold values from -24 to 24
- seq_length: int32 [128], P('ep'), may hold values from 1024 to 16383
- ret_state: float32 [128, 4, 128, 256], P('ep', 'tp'), may hold values from -0.6 to 0.6
- norm_in: float32 [1024], replicated, may hold values from 0.1 to 1.9
- w_query: bfloat16 [1024, 512], P(None, 'tp'), may hold values from -0.1875 to 0.1875
- w_key: bfloat16 [1024, 512], P(None, 'tp'), may hold values from -0.1875 to 0.1875
- w_value: bfloat16 [1024, 1024], P(None, 'tp'), may hold values from -0.1875 to 0.1875
- head_gain: float32 [1024], P('tp'), may hold values from 0.1 to 1.9
- w_output: bfloat16 [1024, 1024], P('tp'), may hold values from -0.1875 to 0.1875
- norm_mid: float32 [1024], replicated, may hold values from 0.1 to 1.9
- route_expert: int32 [128, 2], P('ep'), may hold values from 0 to 3, all different within a row; in each aligned block of 16 rows (0 to 15, 16 to 31, ...) at most 12 rows name the same one
- route_score: float32 [128, 2], P('ep'), may hold values from -6 to 6
- expert_gate: bfloat16 [8, 1024, 1792], P('ep', None, 'tp'), may hold values from -0.1875 to 0.1875
- expert_up: bfloat16 [8, 1024, 1792], P('ep', None, 'tp'), may hold values from -0.1875 to 0.1875
- expert_down: bfloat16 [8, 1792, 1024], P('ep', 'tp'), may hold values from -0.09375 to 0.09375
Outputs:
- mixed: bfloat16 [128, 1024], P('ep', 'tp')
Inputs may be any that keep to these rules, and one draw needn't show every extreme that they name: `route_expert`: each row names 2 different experts; within the rows of one device no expert is named by more than 12 rows, and some device's rows name one expert exactly 12 times.
All inputs are finite; a program needn't handle non-finite values.
Results may differ from a plain program's by a relative error of at most 0.014.
Values may be sent and summed in bfloat16 or wider, within the bound.
A program may use at most 64 MiB of HBM per device.

v0:
```python
import jax
import jax.numpy as jnp
from jax import lax
from jax.sharding import PartitionSpec as P

DK = 128
DV = 256
SPREAD = 2
TOP_K = 2
EPS = 1e-06


def rotate(head_rows, positions):
    half_width = head_rows.shape[-1] // 2
    inverse = 10000.0 ** (-jnp.arange(half_width, dtype=jnp.float32) / half_width)
    angles = positions[:, None] * inverse[None, :]
    cosine = jnp.cos(angles)[:, None, :]
    sine_part = jnp.sin(angles)[:, None, :]
    first_half = head_rows[..., :half_width]
    second = head_rows[..., half_width:]
    return jnp.concatenate(
        [first_half * cosine - second * sine_part, first_half * sine_part + second * cosine],
        axis=-1,
    )


def body(
    tokens,
    seq_length,
    ret_state,
    norm_in,
    w_query,
    w_key,
    w_value,
    head_gain,
    w_output,
    norm_mid,
    route_expert,
    route_score,
    expert_gate,
    expert_up,
    expert_down,
):
    n_lanes = lax.axis_size("tp")
    n_groups = lax.axis_size("ep")
    lane_index = lax.axis_index("tp")
    local_rows = tokens.shape[0]
    width = tokens.shape[1]
    quarter = width // n_lanes
    heads_here = w_query.shape[1] // DK
    token_f = tokens.astype(jnp.float32)
    normed = (
        token_f * lax.rsqrt(jnp.mean(token_f * token_f, axis=-1, keepdims=True) + EPS) * norm_in
    ).astype(jnp.bfloat16)
    query_proj = jnp.dot(normed, w_query, preferred_element_type=jnp.float32).astype(jnp.bfloat16)
    key_proj = jnp.dot(normed, w_key, preferred_element_type=jnp.float32).astype(jnp.bfloat16)
    value_proj = jnp.dot(normed, w_value, preferred_element_type=jnp.float32).astype(jnp.bfloat16)
    positions = seq_length.astype(jnp.float32)
    q_rot = rotate(query_proj.astype(jnp.float32).reshape(local_rows, heads_here, DK), positions)
    k_rot = rotate(
        key_proj.astype(jnp.float32).reshape(local_rows, heads_here, DK), positions
    ) * DK ** (-0.5)
    value_rows = value_proj.astype(jnp.float32).reshape(local_rows, heads_here, DV)
    head_index = (lane_index * heads_here + jnp.arange(heads_here, dtype=jnp.int32)).astype(
        jnp.float32
    )
    decay_rate = 1.0 - jnp.exp2(-2.0 - 2.0 * head_index)
    carried = jnp.einsum("bhd,bhde->bhe", q_rot, ret_state, precision=lax.Precision.HIGHEST)
    within = jnp.sum(q_rot * k_rot, axis=-1, keepdims=True) * value_rows
    retained = decay_rate[None, :, None] * carried + within
    centre = jnp.mean(retained, axis=-1, keepdims=True)
    variance = jnp.mean(jnp.square(retained - centre), axis=-1, keepdims=True)
    ret_out = ((retained - centre) * lax.rsqrt(variance + EPS)).reshape(local_rows, heads_here * DV)
    ret_out = (ret_out * head_gain).astype(jnp.bfloat16)
    partial_value = jnp.dot(ret_out, w_output, preferred_element_type=jnp.float32)
    experts_n = n_groups // SPREAD
    cap = min(local_rows, max(2, 3 * local_rows * TOP_K // (2 * experts_n)))
    flat_rows = route_expert.reshape(-1)
    onehot = (flat_rows[:, None] == jnp.arange(experts_n, dtype=jnp.int32)[None, :]).astype(
        jnp.int32
    )
    rank_index = jnp.sum((jnp.cumsum(onehot, axis=0) - onehot) * onehot, axis=1)
    slot_index = flat_rows * cap + rank_index
    chosen_slot = (
        slot_index[:, None] == jnp.arange(experts_n * cap, dtype=jnp.int32)[None, :]
    ).astype(jnp.float32)
    chosen_slot = chosen_slot.reshape(local_rows, TOP_K, experts_n * cap)
    placing = jnp.sum(chosen_slot, axis=1).astype(jnp.bfloat16)
    weights = jax.nn.softmax(route_score, axis=-1)
    combine = jnp.sum(chosen_slot * weights[:, :, None], axis=1)
    gate_rows = expert_gate[0]
    up_rows = expert_up[0]
    down_rows = expert_down[0]
    attended = lax.psum(partial_value.astype(jnp.bfloat16), "tp").astype(jnp.float32)
    resid_full = (token_f + attended).astype(jnp.bfloat16)
    resid_f = resid_full.astype(jnp.float32)
    mid_full = (
        resid_f * lax.rsqrt(jnp.mean(resid_f * resid_f, axis=-1, keepdims=True) + EPS) * norm_mid
    ).astype(jnp.bfloat16)
    resid = lax.dynamic_slice_in_dim(resid_full, lane_index * quarter, quarter, 1)
    mid = lax.dynamic_slice_in_dim(mid_full, lane_index * quarter, quarter, 1)
    packed = jnp.einsum("re,rc->ec", placing, mid, preferred_element_type=jnp.float32).astype(
        jnp.bfloat16
    )
    packed = packed.reshape(experts_n, cap, quarter)
    send_buffer = jnp.repeat(packed, SPREAD, axis=0)
    received = lax.all_to_all(send_buffer, "ep", split_axis=0, concat_axis=0, tiled=True)
    groups, row_count, cols = received.shape
    piece_cols = lax.all_gather(received, "tp", axis=2, tiled=True)
    piece_width = piece_cols.shape[2]
    flat_in = piece_cols.reshape(groups * row_count, piece_width)
    gate_sum = jnp.dot(flat_in, gate_rows, preferred_element_type=jnp.float32)
    up_sum = jnp.dot(flat_in, up_rows, preferred_element_type=jnp.float32)
    hidden = (jax.nn.silu(gate_sum) * up_sum).astype(jnp.bfloat16)
    down_part = jnp.dot(hidden, down_rows, preferred_element_type=jnp.float32)
    share = lax.psum_scatter(
        down_part.astype(jnp.bfloat16), "tp", scatter_dimension=1, tiled=True
    ).astype(jnp.float32)
    returned = share.astype(jnp.bfloat16).reshape(groups, row_count, share.shape[1])
    arrived = lax.all_to_all(returned, "ep", split_axis=0, concat_axis=0, tiled=True)
    part_total = jnp.sum(
        arrived.reshape(experts_n, SPREAD, cap, quarter).astype(jnp.float32), axis=1
    )
    expert_out = part_total.astype(jnp.bfloat16)
    expert_mix = jnp.dot(
        combine,
        expert_out.reshape(experts_n * cap, quarter).astype(jnp.float32),
        precision=lax.Precision.HIGHEST,
    )
    return (resid.astype(jnp.float32) + expert_mix).astype(jnp.bfloat16)


def solution(mesh):
    placed = (
        P("ep", None),
        P("ep"),
        P("ep", "tp", None, None),
        P(),
        P(None, "tp"),
        P(None, "tp"),
        P(None, "tp"),
        P("tp"),
        P("tp", None),
        P(),
        P("ep", None),
        P("ep", None),
        P("ep", None, "tp"),
        P("ep", None, "tp"),
        P("ep", "tp", None),
    )
    return jax.shard_map(body, mesh=mesh, in_specs=placed, out_specs=P("ep", "tp"), check_vma=False)
```

profile of v0, /device:TPU:0, one launch (start us, length us, event | category | flops | bytes accessed | tf_op | source)
XLA Modules:
  0.0 89.4 jit_solution(11786482664120521328)
XLA Ops:
  6.5 0.0 copy-start
  6.5 0.0 copy-start.3
  6.5 0.0 copy-start.7
  6.5 0.0 copy-start.5
  6.5 0.0 reduce-scatter.2.cloned.1.call-start
  6.7 0.8 reduce_max.9
  7.5 0.7 fusion.51
  8.2 0.7 fusion.50
  8.9 0.7 convert_element_type.79
  9.5 0.9 fusion.22
  10.4 0.0 copy-start.4
  10.4 1.2 %fusion.10 = f32[16,1,128]{2,0,1:T(8,128)S(1)} fusion(bf16[1024,128]{1,0:T(8,128)(2,1)} %param.20, bf16[16,1024]{1,0:T(8,128)(2,1)} %param.15, f32[1024]{0:T(1024)} %param.18, f32[16]{0:T(128)S(1)} %add_rsqrt_fusion.2), kind=kOutput, calls=%fused_computation.18 | convolution fusion | flops 4263936 | bytes 307264 | tf_op jit(solution)/shard_map/dot_general | solution.py:56
  11.6 1.2 %fusion.8 = f32[16,1,128]{2,0,1:T(8,128)S(1)} fusion(bf16[1024,128]{1,0:T(8,128)(2,1)} %param.19, bf16[16,1024]{1,0:T(8,128)(2,1)} %param.15, f32[1024]{0:T(1024)} %param.18, f32[16]{0:T(128)S(1)} %add_rsqrt_fusion.2), kind=kOutput, calls=%fused_computation.16 | convolution fusion | flops 4263936 | bytes 307264 | tf_op jit(solution)/shard_map/dot_general | solution.py:55
  12.8 0.8 copy.28
  13.6 0.1 eq.29
  13.7 0.0 copy-start.6
  13.7 0.0 copy-start.2
  13.7 0.1 fusion.37
  13.8 0.2 fusion.45
  14.0 0.0 copy-done
  14.0 0.0 copy-start.1
  14.0 1.1 %fusion = f32[16,1,256]{2,1,0:T(1,128)S(1)} fusion(f32[16,128,1]{1,2,0:T(1,128)S(1)} %bitcast.45, f32[16,1,128,256]{3,2,1,0:T(8,128)S(1)} %copy-done), kind=kOutput, calls=%fused_computation | convolution fusion | flops 6291456 | bytes 2121728 | tf_op jit(solution)/shard_map/bhd,bhde->bhe/dot_general | solution.py:68
  15.1 0.0 copy-done.3
  15.1 0.0 copy-done.7
  15.1 0.0 copy-done.6
  15.2 0.3 fusion.58
  15.5 0.2 multiply_reduce_fusion.1
  15.7 0.0 copy-done.5
  15.7 0.0 copy-done.2
  15.7 0.2 convolution_convert_fusion.1
  15.9 12.9 %psum.7 = bf16[16,1024]{1,0:T(8,128)(2,1)S(1)} all-reduce(bf16[16,1024]{1,0:T(8,128)(2,1)S(1)} %convolution_convert_fusion.1), channel_id=1, replica_groups=mesh['ep'=8,'tp'=4] {'tp'}, use_global_device_ids=true, to_apply=%region_4.0 | all-reduce | flops 16384 | bytes 65536 | tf_op jit(solution)/shard_map/psum | solution.py:94
  28.8 0.1 multiply_reduce_fusion
  29.0 0.1 fusion.28
  29.0 0.1 reduce_window_sum.11
  29.1 0.2 select_reduce_fusion.1
  29.3 0.1 reduce_sum.100
  29.4 0.1 copy.29
  29.5 0.0 copy-done.4
  29.5 0.8 dynamic-slice
  30.3 0.1 convert_reduce_fusion
  30.3 0.2 convolution_convert_fusion.2
  30.6 12.5 %all_to_all.10 = bf16[8,12,256]{2,1,0:T(8,128)(2,1)S(1)} all-to-all(bf16[8,12,256]{2,1,0:T(8,128)(2,1)S(1)} %bitcast.44), channel_id=1, replica_groups=mesh['ep'=8,'tp'=4] {'ep'}, dimensions={0} | all-to-all | bytes 98304 | tf_op jit(solution)/shard_map/all_to_all | solution.py:107
  43.1 5.8 %all_gather.3 = bf16[8,12,1024]{2,1,0:T(8,128)(2,1)S(1)} all-gather(bf16[8,12,256]{2,1,0:T(8,128)(2,1)S(1)} %all_to_all.10), channel_id=1, replica_groups=mesh['ep'=8,'tp'=4] {'tp'}, dimensions={2}, use_global_device_ids=true | all-gather | bytes 245760 | tf_op jit(solution)/shard_map/all_gather | solution.py:109
  48.9 0.0 copy-done.1
  48.9 0.4 fusion.14
  49.4 2.8 %convolution_convert_fusion = bf16[96,1024]{1,0:T(8,128)(2,1)} fusion(bf16[96,1024]{1,0:T(8,128)(2,1)S(1)} %reshape.273, bf16[1,448,1024]{2,1,0:T(8,128)(2,1)} %param.29, bf16[1,1024,448]{1,2,0:T(8,128)(2,1)} %param.28, f32[96,448]{1,0:T(8,128)S(1)} %fusion.14), kind=kOutput, calls=%fused_computation.2 | convolution fusion | flops 176517120 | bytes 2400256 | tf_op jit(solution)/shard_map/dot_general | solution.py:115
  52.2 0.0 reduce-scatter.2.cloned.1.call-update
  52.2 16.5 %reduce-scatter.2.cloned.1.call-done = bf16[96,256]{1,0:T(8,128)(2,1)} async-done(((bf16[96,1024]{1,0:T(8,128)(2,1)}), bf16[96,256]{1,0:T(8,128)(2,1)}) %reduce-scatter.2.cloned.1.call-update) | async-done | bytes 49168 | tf_op jit(solution)/shard_map/reduce_scatter | solution.py:116
  68.7 0.8 reshape.274
  69.5 12.2 %all_to_all.11 = bf16[8,12,256]{2,1,0:T(8,128)(2,1)S(1)} all-to-all(bf16[8,12,256]{2,1,0:T(8,128)(2,1)S(1)} %reshape.274), channel_id=1, replica_groups=mesh['ep'=8,'tp'=4] {'ep'}, dimensions={0} | all-to-all | bytes 98304 | tf_op jit(solution)/shard_map/all_to_all | solution.py:120
  81.8 0.7 fusion.3
  (12 shorter events, 0.2 us)
Async XLA Ops:
  6.5 7.5 %copy-start = (f32[16,1,128,256]{3,2,1,0:T(8,128)S(1)}, f32[16,1,128,256]{3,2,1,0:T(8,128)}, u32[]{:S(2)}) copy-start(f32[16,1,128,256]{3,2,1,0:T(8,128)} %param.17) | copy-start | bytes 6291460
  6.5 8.6 %copy-start.3 = (bf16[16,1024]{1,0:T(8,128)(2,1)S(1)}, bf16[16,1024]{1,0:T(8,128)(2,1)}, u32[]{:S(2)}) copy-start(bf16[16,1024]{1,0:T(8,128)(2,1)} %param.15) | copy-start | bytes 98308
  6.5 8.6 %copy-start.7 = (f32[1024]{0:T(1024)S(1)}, f32[1024]{0:T(1024)}, u32[]{:S(2)}) copy-start(f32[1024]{0:T(1024)} %param.18) | copy-start | bytes 12292
  6.5 9.2 %copy-start.5 = (f32[256]{0:T(256)S(1)}, f32[256]{0:T(256)}, u32[]{:S(2)}) copy-start(f32[256]{0:T(256)} %param.22) | copy-start | bytes 3076
  6.5 62.2 %reduce-scatter.2.cloned.1.call-start = ((), (), s32[]{:S(2)}) async-start(), calls=%async_computation.3 | async-start | bytes 245760 | tf_op jit(solution)/shard_map/reduce_scatter | solution.py:116
  10.4 19.1 %copy-start.4 = (s32[16,2]{0,1:T(2,128)S(1)}, s32[16,2]{0,1:T(2,128)}, u32[]{:S(2)}) copy-start(s32[16,2]{0,1:T(2,128)} %param.25) | copy-start | bytes 388
  13.7 1.5 %copy-start.6 = (bf16[1024,256]{1,0:T(8,128)(2,1)S(1)}, bf16[1024,256]{1,0:T(8,128)(2,1)}, u32[]{:S(2)}) copy-start(bf16[1024,256]{1,0:T(8,128)(2,1)} %param.21) | copy-start | bytes 1572868
  13.7 2.0 %copy-start.2 = (bf16[256,1024]{1,0:T(8,128)(2,1)S(1)}, bf16[256,1024]{1,0:T(8,128)(2,1)}, u32[]{:S(2)}) copy-start(bf16[256,1024]{1,0:T(8,128)(2,1)} %param.23) | copy-start | bytes 1572868
  14.0 34.9 %copy-start.1 = (bf16[1,1024,448]{1,2,0:T(8,128)(2,1)S(1)}, bf16[1,1024,448]{1,2,0:T(8,128)(2,1)}, u32[]{:S(2)}) copy-start(bf16[1,1024,448]{1,2,0:T(8,128)(2,1)} %param.27) | copy-start | bytes 2752516
Sparse Core Ops, SparseCore 0:
  52.3 16.3 reduce-scatter.1
where the time goes:
time: 89.9 us; the launch traced here: 89.4 us
  blocking collectives  43.4 us (48%)
  waiting for transfers between devices  16.5 us (18%)
  between operations  13.6 us (15%)
  matrix products  8.21 us (9%)
  other arithmetic  4.82 us (5%)
  local copies, waits for them, and re-layouts  2.74 us (3%)
    reduce_scatter x1, waiting for transfers between devices, body(): lax.psum_scatter(down_part.astype(jnp.bfloat16), 'tp', scatter_dimension=...  16.5 us
    psum x1, blocking collectives, body(): lax.psum(partial_value.astype(jnp.bfloat16), 'tp').astype(jnp.float32)  12.9 us
    all_to_all x1, blocking collectives, body(): lax.all_to_all(send_buffer, 'ep', split_axis=0, concat_axis=0, tiled=True)  12.5 us
    all_to_all x1, blocking collectives, body(): lax.all_to_all(returned, 'ep', split_axis=0, concat_axis=0, tiled=True)  12.2 us
    all_gather x1, blocking collectives, body(): piece_cols = lax.all_gather(received, 'tp', axis=2, tiled=True)  5.76 us
    dot_general x1, matrix products, body(): down_part = jnp.dot(hidden, down_rows, preferred_element_type=jnp.float32)  2.82 us
  transfers between devices with their start and end apart: 1, of which 1 were waited for; matrix products, arithmetic and copies ran while one was open for 0% of the time, Pallas kernels for 0%

commit v1 on v0

--- a/solution.py
+++ b/solution.py
@@ -91,7 +91,9 @@
     gate_rows = expert_gate[0]
     up_rows = expert_up[0]
     down_rows = expert_down[0]
-    attended = lax.psum(partial_value.astype(jnp.bfloat16), "tp").astype(jnp.float32)
+    attended = jnp.sum(lax.all_gather(partial_value.astype(jnp.bfloat16), "tp"), axis=0).astype(
+        jnp.float32
+    )
     resid_full = (token_f + attended).astype(jnp.bfloat16)
     resid_f = resid_full.astype(jnp.float32)
     mid_full = (

time: 89.9 us -> 96.2 us (1.070)
  other arithmetic: 4.82 us -> 11.8 us
  blocking collectives: 43.4 us -> 37.4 us
  local copies, waits for them, and re-layouts: 2.74 us -> 6.26 us
  waiting for transfers between devices: 16.5 us -> 17.5 us
    psum x1 -> x0, blocking collectives: 12.9 us -> none  [body(): lax.psum(partial_value.astype(jnp.bfloat16), 'tp').astype(jnp.float32)]
    all_gather x0 -> x1, blocking collectives: none -> 6.51 us  [body(): lax.all_gather(partial_value.astype(jnp.bfloat16), 'tp')]
    reduce_sum x2, local copies, waits for them, and re-layouts: 0.17 us -> 2.64 us  [body(): rank_index = jnp.sum((jnp.cumsum(onehot, axis=0) - onehot) * onehot, axis=1)]
    another operation x1, other arithmetic: 0.06 us -> 1.35 us  [body(): rank_index = jnp.sum((jnp.cumsum(onehot, axis=0) - onehot) * onehot, axis=1)]
    add x1, other arithmetic: 0.01 us -> 1.25 us  [body(): slot_index = flat_rows * cap + rank_index]
    reduce_sum x1, other arithmetic: 0.18 us -> 1.41 us  [body(): rank_index = jnp.sum((jnp.cumsum(onehot, axis=0) - onehot) * onehot, axis=1)]
where the time goes in v1:
time: 96.2 us; the launch traced here: 95.4 us
  blocking collectives  37.4 us (39%)
  waiting for transfers between devices  17.5 us (18%)
  between operations  13.6 us (14%)
  other arithmetic  11.8 us (12%)
  matrix products  8.87 us (9%)
  local copies, waits for them, and re-layouts  6.26 us (7%)
    reduce_scatter x1, waiting for transfers between devices, body(): lax.psum_scatter(down_part.astype(jnp.bfloat16), 'tp', scatter_dimension=...  17.5 us
    all_to_all x1, blocking collectives, body(): lax.all_to_all(send_buffer, 'ep', split_axis=0, concat_axis=0, tiled=True)  12.9 us
    all_to_all x1, blocking collectives, body(): lax.all_to_all(returned, 'ep', split_axis=0, concat_axis=0, tiled=True)  12.2 us
    all_gather x1, blocking collectives, body(): lax.all_gather(partial_value.astype(jnp.bfloat16), 'tp')  6.51 us
    all_gather x1, blocking collectives, body(): piece_cols = lax.all_gather(received, 'tp', axis=2, tiled=True)  5.76 us
    dot_general x1, matrix products, body(): down_part = jnp.dot(hidden, down_rows, preferred_element_type=jnp.float32)  2.81 us
    reduce_sum x2, local copies, waits for them, and re-layouts, body(): rank_index = jnp.sum((jnp.cumsum(onehot, axis=0) - onehot) * onehot, axis=1)  2.64 us
  transfers between devices with their start and end apart: 1, of which 1 were waited for; matrix products, arithmetic and copies ran while one was open for 0% of the time, Pallas kernels for 0%

profile of v1, /device:TPU:0, one launch (start us, length us, event | category | flops | bytes accessed | tf_op | source)
XLA Modules:
  0.0 95.4 jit_solution(1410387260833597594)
XLA Ops:
  6.5 0.0 copy-start
  6.5 0.0 copy-start.2
  6.5 0.0 reduce-scatter.2.cloned.1.call-start
  6.6 0.8 reduce_max.9
  7.5 0.7 fusion.51
  8.2 1.3 %fusion.50 = f32[16,2]{0,1:T(2,128)} fusion(f32[16,2]{0,1:T(2,128)} %param.26, f32[16]{0:T(128)S(1)} %fusion.51, f32[16]{0:T(128)S(1)} %reduce_max.9), kind=kLoop, calls=%fused_computation.76 | loop fusion | flops 64 | bytes 384 | tf_op jit(solution)/shard_map/div | solution.py:89
  9.4 0.7 convert_element_type.81
  10.1 0.9 fusion.22
  11.0 0.0 copy-start.8
  11.0 1.2 %fusion.10 = f32[16,1,128]{2,0,1:T(8,128)S(1)} fusion(bf16[1024,128]{1,0:T(8,128)(2,1)} %param.20, bf16[16,1024]{1,0:T(8,128)(2,1)} %param.15, f32[1024]{0:T(1024)} %param.18, f32[16]{0:T(128)S(1)} %add_rsqrt_fusion.2), kind=kOutput, calls=%fused_computation.18 | convolution fusion | flops 4263936 | bytes 307264 | tf_op jit(solution)/shard_map/dot_general | solution.py:56
  12.1 0.0 copy-done.8
  12.1 1.2 %fusion.8 = f32[16,1,128]{2,0,1:T(8,128)S(1)} fusion(bf16[1024,128]{1,0:T(8,128)(2,1)} %param.19, bf16[16,1024]{1,0:T(8,128)(2,1)} %param.15, f32[1024]{0:T(1024)} %param.18, f32[16]{0:T(128)S(1)} %add_rsqrt_fusion.2), kind=kOutput, calls=%fused_computation.16 | convolution fusion | flops 4263936 | bytes 307264 | tf_op jit(solution)/shard_map/dot_general | solution.py:55
  13.3 0.8 copy.28
  14.1 0.6 eq.29
  14.7 0.0 copy-start.3
  14.7 0.0 copy-start.6
  14.7 0.0 copy-start.7
  14.7 0.0 copy-start.9
  14.7 0.0 copy-start.4
  14.7 0.1 fusion.37
  14.9 0.2 fusion.45
  15.1 0.0 copy-done
  15.1 0.0 copy-start.1
  15.1 1.1 %fusion = f32[16,1,256]{2,1,0:T(1,128)S(1)} fusion(f32[16,128,1]{1,2,0:T(1,128)S(1)} %bitcast.47, f32[16,1,128,256]{3,2,1,0:T(8,128)S(1)} %copy-done), kind=kOutput, calls=%fused_computation | convolution fusion | flops 6291456 | bytes 2121728 | tf_op jit(solution)/shard_map/bhd,bhde->bhe/dot_general | solution.py:68
  16.2 0.0 copy-done.3
  16.2 0.0 copy-done.6
  16.2 0.0 copy-done.7
  16.2 0.0 copy-done.9
  16.2 0.3 fusion.58
  16.5 0.0 copy-start.5
  16.6 0.5 copy-done.5
  17.1 0.2 multiply_reduce_fusion.1
  17.3 0.6 add_rsqrt_fusion.1
  17.9 0.0 copy-done.4
  17.9 0.7 fusion.28
  18.5 1.4 %reduce_window_sum.11 = s32[32,4]{1,0:T(8,128)} reduce-window(s32[32,4]{1,0:T(8,128)} %fusion.28, s32[]{:T(128)} %constant.51.clone.1), window={size=32x1 pad=31_0x0_0}, to_apply=%region_5.6 | reduce-window | flops 3968 | bytes 1028 | tf_op jit(solution)/shard_map/jit(cumsum)/reduce_window_sum | solution.py:82
  19.9 1.4 %select_reduce_fusion.1 = s32[32]{0:T(128)} fusion(s32[32,4]{1,0:T(8,128)} %reduce_window_sum.11, s32[32]{0:T(128)} %eq.29), kind=kLoop, calls=%fused_computation.45 | loop fusion | flops 608 | bytes 768 | tf_op jit(solution)/shard_map/reduce_sum | solution.py:82
  21.3 1.3 %reduce_sum.113 = s32[16,2]{1,0:T(8,128)} reshape(s32[32]{0:T(128)} %select_reduce_fusion.1) | data formatting | bytes 256 | tf_op jit(solution)/shard_map/reduce_sum | solution.py:82
  22.6 1.4 %copy.29 = s32[16,2]{0,1:T(2,128)} copy(s32[16,2]{1,0:T(8,128)} %reduce_sum.113) | data formatting | bytes 256 | tf_op jit(solution)/shard_map/reduce_sum | solution.py:82
  23.9 1.2 %multiply_add_fusion = s32[16,2]{0,1:T(2,128)} fusion(s32[16,2]{0,1:T(2,128)} %copy.29, s32[16,2]{0,1:T(2,128)} %param.25), kind=kLoop, calls=%fused_computation.75 | loop fusion | flops 64 | bytes 384 | tf_op jit(solution)/shard_map/add | solution.py:83
  25.2 0.0 copy-done.2
  25.2 0.9 convolution_convert_fusion.1
  26.1 6.5 %all-gather = bf16[64,1024]{1,0:T(8,128)(2,1)S(1)} all-gather(bf16[16,1024]{1,0:T(8,128)(2,1)S(1)} %convolution_convert_fusion.1), channel_id=2, replica_groups=mesh['ep'=8,'tp'=4] {'tp'}, dimensions={0}, use_global_device_ids=true | all-gather | bytes 163840 | tf_op jit(solution)/shard_map/all_gather | solution.py:94
  32.6 0.9 multiply_reduce_fusion
  33.5 0.8 dynamic-slice
  34.3 0.8 convert_reduce_fusion
  35.1 0.2 convolution_convert_fusion.2
  35.3 12.9 %all_to_all.10 = bf16[8,12,256]{2,1,0:T(8,128)(2,1)S(1)} all-to-all(bf16[8,12,256]{2,1,0:T(8,128)(2,1)S(1)} %bitcast.46), channel_id=1, replica_groups=mesh['ep'=8,'tp'=4] {'ep'}, dimensions={0} | all-to-all | bytes 98304 | tf_op jit(solution)/shard_map/all_to_all | solution.py:109
  48.2 5.8 %all_gather.11 = bf16[8,12,1024]{2,1,0:T(8,128)(2,1)S(1)} all-gather(bf16[8,12,256]{2,1,0:T(8,128)(2,1)S(1)} %all_to_all.10), channel_id=1, replica_groups=mesh['ep'=8,'tp'=4] {'tp'}, dimensions={2}, use_global_device_ids=true | all-gather | bytes 245760 | tf_op jit(solution)/shard_map/all_gather | solution.py:111
  54.0 0.0 copy-done.1
  54.0 0.4 fusion.14
  54.5 2.8 %convolution_convert_fusion = bf16[96,1024]{1,0:T(8,128)(2,1)} fusion(bf16[96,1024]{1,0:T(8,128)(2,1)S(1)} %reshape.273, bf16[1,448,1024]{2,1,0:T(8,128)(2,1)} %param.29, bf16[1,1024,448]{1,2,0:T(8,128)(2,1)} %param.28, f32[96,448]{1,0:T(8,128)S(1)} %fusion.14), kind=kOutput, calls=%fused_computation.2 | convolution fusion | flops 176517120 | bytes 2400256 | tf_op jit(solution)/shard_map/dot_general | solution.py:117
  57.3 0.0 reduce-scatter.2.cloned.1.call-update
  57.3 17.5 %reduce-scatter.2.cloned.1.call-done = bf16[96,256]{1,0:T(8,128)(2,1)} async-done(((bf16[96,1024]{1,0:T(8,128)(2,1)}), bf16[96,256]{1,0:T(8,128)(2,1)}) %reduce-scatter.2.cloned.1.call-update) | async-done | bytes 49168 | tf_op jit(solution)/shard_map/reduce_scatter | solution.py:118
  74.8 0.8 reshape.274
  75.6 12.2 %all_to_all.11 = bf16[8,12,256]{2,1,0:T(8,128)(2,1)S(1)} all-to-all(bf16[8,12,256]{2,1,0:T(8,128)(2,1)S(1)} %reshape.274), channel_id=1, replica_groups=mesh['ep'=8,'tp'=4] {'ep'}, dimensions={0} | all-to-all | bytes 98304 | tf_op jit(solution)/shard_map/all_to_all | solution.py:122
  87.8 0.7 fusion.3
  (11 shorter events, 0.2 us)
Async XLA Ops:
  6.5 8.5 %copy-start = (f32[16,1,128,256]{3,2,1,0:T(8,128)S(1)}, f32[16,1,128,256]{3,2,1,0:T(8,128)}, u32[]{:S(2)}) copy-start(f32[16,1,128,256]{3,2,1,0:T(8,128)} %param.17) | copy-start | bytes 6291460
  6.5 18.7 %copy-start.2 = (bf16[256,1024]{1,0:T(8,128)(2,1)S(1)}, bf16[256,1024]{1,0:T(8,128)(2,1)}, u32[]{:S(2)}) copy-start(bf16[256,1024]{1,0:T(8,128)(2,1)} %param.23) | copy-start | bytes 1572868
  6.5 68.2 %reduce-scatter.2.cloned.1.call-start = ((), (), s32[]{:S(2)}) async-start(), calls=%async_computation.3 | async-start | bytes 245760 | tf_op jit(solution)/shard_map/reduce_scatter | solution.py:118
  11.0 1.2 %copy-start.8 = (f32[16]{0:T(128)}, f32[16]{0:T(128)S(1)}, u32[]{:S(2)}) copy-start(f32[16]{0:T(128)S(1)} %add_rsqrt_fusion.2) | copy-start | bytes 196
  14.7 1.5 %copy-start.3 = (bf16[16,1024]{1,0:T(8,128)(2,1)S(1)}, bf16[16,1024]{1,0:T(8,128)(2,1)}, u32[]{:S(2)}) copy-start(bf16[16,1024]{1,0:T(8,128)(2,1)} %param.15) | copy-start | bytes 98308
  14.7 1.5 %copy-start.6 = (bf16[1024,256]{1,0:T(8,128)(2,1)S(1)}, bf16[1024,256]{1,0:T(8,128)(2,1)}, u32[]{:S(2)}) copy-start(bf16[1024,256]{1,0:T(8,128)(2,1)} %param.21) | copy-start | bytes 1572868
  14.7 1.5 %copy-start.7 = (f32[1024]{0:T(1024)S(1)}, f32[1024]{0:T(1024)}, u32[]{:S(2)}) copy-start(f32[1024]{0:T(1024)} %param.18) | copy-start | bytes 12292
  14.7 1.5 %copy-start.9 = (f32[16]{0:T(128)S(1)}, f32[16]{0:T(128)}, u32[]{:S(2)}) copy-start(f32[16]{0:T(128)} %copy-done.8) | copy-start | bytes 196
  14.7 3.1 %copy-start.4 = (s32[32]{0:T(128)S(1)}, s32[32]{0:T(128)}, u32[]{:S(2)}) copy-start(s32[32]{0:T(128)} %eq.29) | copy-start | bytes 388
  15.1 39.0 %copy-start.1 = (bf16[1,1024,448]{1,2,0:T(8,128)(2,1)S(1)}, bf16[1,1024,448]{1,2,0:T(8,128)(2,1)}, u32[]{:S(2)}) copy-start(bf16[1,1024,448]{1,2,0:T(8,128)(2,1)} %param.27) | copy-start | bytes 2752516
  16.5 0.5 copy-start.5
Sparse Core Ops, SparseCore 0:
  57.4 17.3 reduce-scatter.1
